TPU v7x, 256 devices: a 4x2x16 block of a 4x16x16 slice. The times are simulated.
256 devices in a mesh: grp: 2 (over y), sp: 32 (over z, core), tp: 4 (over x).
Axes of the slice: x: 4, y: 2, z: 16, core: 2. Of those that a mesh axis runs over, the one named last changes fastest.
The devices are a block of a 4x16x16 slice.
Arguments:
- conv_value: bfloat16 [32768, 1024], P(('grp', 'sp'), 'tp'), parts along dimension 0, may hold values from -6 to 6
- conv_gate: bfloat16 [32768, 1024], P(('grp', 'sp'), 'tp'), parts along dimension 0, may hold values from -6 to 6
- kernel: bfloat16 [31, 1024], P(None, 'tp'), may hold values from -4 to 4
- conv_bias: float32 [1024], P('tp'), may hold values from -3 to 3
- ln_gain: float32 [1024], P('tp'), may hold values from 0.1 to 1.9
- ln_bias: float32 [1024], P('tp'), may hold values from -3 to 3
- out_gain: float32 [1024], P('tp'), may hold values from 0.1 to 1.9
- out_weight: bfloat16 [1024, 2048], replicated, may hold values from -0.1875 to 0.1875
- residual: bfloat16 [32768, 2048], P(('grp', 'sp', 'tp')), parts along dimension 0, may hold values from -6 to 6
- moe_gain: float32 [2048], replicated, may hold values from 0.1 to 1.9
- expert_ids: int32 [32768, 2], P(('grp', 'sp', 'tp')), parts along dimension 0, may hold values from 0 to 127, as said below
- expert_weights: float32 [32768, 2], P(('grp', 'sp', 'tp')), parts along dimension 0, may hold values from 0.1 to 0.7
- w_gate: bfloat16 [128, 2048, 512], P(('sp', 'tp')), may hold values from -0.125 to 0.125
- w_up: bfloat16 [128, 2048, 512], P(('sp', 'tp')), may hold values from -0.125 to 0.125
- w_down: bfloat16 [128, 512, 2048], P(('sp', 'tp')), may hold values from -0.25 to 0.25
Outputs:
- layer_out: bfloat16 [32768, 2048], P(('grp', 'sp', 'tp')), parts along dimension 0
There are 2 independent parts, one for each index of `grp`. A program takes and returns all parts, laid end to end along the dimension named above; an argument that names none is the same for every part. Nothing has to cross between parts.
Inputs may be any that keep to these rules, and one draw needn't show every extreme that they name: `expert_ids`: each row names two different experts of one group (group = expert number // 32). Among the 128 rows of one device (aligned blocks of 128 rows) no expert is named more than 4 times, and in every such block some expert is named exactly 4 times.
All inputs are finite; a program needn't handle non-finite values.
Results may differ from a plain program's by a relative error of at most 0.0095.
Values may be sent and summed in bfloat16 or wider, within the bound.
A program may use at most 64 MiB of HBM per device.

v0:
```python
import jax
import jax.numpy as jnp
from jax import lax
from jax.sharding import PartitionSpec as P

EPSILON = 1e-06


def passed_along(block, axis, distance):
    devices = range(lax.axis_size(axis))
    route = [(i - distance, i) for i in devices if i - distance in devices]
    return lax.ppermute(block, axis, route)


def copy_for_each(shard, axis):
    size = lax.axis_size(axis)
    return lax.all_to_all(
        jnp.broadcast_to(shard[None], (size, *shard.shape)), axis, 0, 0, tiled=True
    )


def of_everyone(shard, axis):
    return copy_for_each(shard, axis).sum(axis=0)


def together(arrays, axis):
    ends = [0]
    for a in arrays:
        ends.append(ends[-1] + a.size)
    subtotal = of_everyone(jnp.concatenate([a.ravel() for a in arrays]), axis)
    return tuple((subtotal[b:e].reshape(a.shape) for a, b, e in zip(arrays, ends, ends[1:])))


def per_device(
    conv_value,
    conv_gate,
    kernel,
    conv_bias,
    ln_gain,
    ln_bias,
    out_gain,
    out_weight,
    residual,
    moe_gain,
    expert_ids,
    expert_weights,
    w_gate,
    w_up,
    w_down,
):
    tok_rows, channels = conv_value.shape
    reach_rows = kernel.shape[0] - 1
    full_channels = channels * lax.axis_size("tp")
    gated = (conv_value.astype(jnp.float32) * jax.nn.sigmoid(conv_gate.astype(jnp.float32))).astype(
        jnp.bfloat16
    )
    before = passed_along(gated[tok_rows - reach_rows :], "sp", 1)
    padded = jnp.concatenate([before, gated], axis=0)
    convolved = jnp.zeros((tok_rows, channels), jnp.float32) + conv_bias
    for offset in range(reach_rows + 1):
        convolved = convolved + padded[offset : offset + tok_rows].astype(jnp.float32) * kernel[
            offset
        ].astype(jnp.float32)
    totals = together((jnp.sum(convolved, axis=1), jnp.sum(convolved * convolved, axis=1)), "tp")
    average = (totals[0] / full_channels)[:, None]
    spread = (totals[1] / full_channels)[:, None] - average * average
    swished = jax.nn.silu((convolved - average) * lax.rsqrt(spread + EPSILON) * ln_gain + ln_bias)
    energy = of_everyone(jnp.sum(swished * swished, axis=1), "tp")
    branch = (swished * lax.rsqrt(energy / full_channels + EPSILON)[:, None] * out_gain).astype(
        jnp.bfloat16
    )
    row_count = tok_rows // lax.axis_size("tp")
    regrouped = lax.all_to_all(branch, "tp", split_axis=0, concat_axis=1, tiled=True)
    projected = jnp.dot(regrouped, out_weight, preferred_element_type=jnp.float32)
    hidden = (residual.astype(jnp.float32) + projected).astype(jnp.bfloat16)
    widened = hidden.astype(jnp.float32)
    normed = (
        widened * lax.rsqrt(jnp.mean(widened * widened, axis=1, keepdims=True) + EPSILON) * moe_gain
    ).astype(jnp.bfloat16)
    width = normed.shape[1]
    experts = lax.axis_size("sp") * lax.axis_size("tp")
    capacity = 2 * row_count // min(row_count, experts // 2)
    flat_ids = expert_ids.reshape(-1)
    onehot = (flat_ids[:, None] == jnp.arange(experts, dtype=jnp.int32)[None, :]).astype(jnp.int32)
    slot_rank = jnp.sum((jnp.cumsum(onehot, axis=0) - 1) * onehot, axis=1)
    position = flat_ids * capacity + slot_rank
    outgoing = (
        jnp.zeros((experts * capacity, width), jnp.bfloat16)
        .at[position]
        .set(jnp.repeat(normed, 2, axis=0))
    )
    outgoing = outgoing.reshape(experts, capacity, width)
    arriving = lax.all_to_all(outgoing, ("sp", "tp"), split_axis=0, concat_axis=0, tiled=True)
    flattened = arriving.reshape(-1, width)
    gate_part = jnp.dot(flattened, w_gate[0], preferred_element_type=jnp.float32)
    up_part = jnp.dot(flattened, w_up[0], preferred_element_type=jnp.float32)
    active = (jax.nn.silu(gate_part) * up_part).astype(jnp.bfloat16)
    result = jnp.dot(active, w_down[0], preferred_element_type=jnp.float32).astype(jnp.bfloat16)
    produced = result.reshape(arriving.shape)
    returned = lax.all_to_all(produced, ("sp", "tp"), split_axis=0, concat_axis=0, tiled=True)
    returned = returned.reshape(experts * capacity, width)
    picked = returned[position].reshape(row_count, 2, width)
    combined = jnp.sum(picked.astype(jnp.float32) * expert_weights[:, :, None], axis=1)
    return (widened + combined).astype(jnp.bfloat16)


def solution(mesh):
    in_specs = (
        P(("grp", "sp"), "tp"),
        P(("grp", "sp"), "tp"),
        P(None, "tp"),
        P("tp"),
        P("tp"),
        P("tp"),
        P("tp"),
        P(),
        P(("grp", "sp", "tp"), None),
        P(),
        P(("grp", "sp", "tp"), None),
        P(("grp", "sp", "tp"), None),
        P(("sp", "tp"), None, None),
        P(("sp", "tp"), None, None),
        P(("sp", "tp"), None, None),
    )
    out_specs = P(("grp", "sp", "tp"), None)
    return jax.shard_map(
        per_device, mesh=mesh, in_specs=in_specs, out_specs=out_specs, check_vma=False
    )
```

profile of v0, /device:TPU:33, one launch (start us, length us, event | category | flops | bytes accessed | tf_op | source)
XLA Modules:
  0.0 328.9 jit_solution(4955386901156573632)
XLA Ops:
  0.0 1.3 multiply_convert_fusion.2
  1.4 5.7 %collective-permute-start = (bf16[30,256]{1,0:T(8,128)(2,1)S(1)}, bf16[30,256]{1,0:T(8,128)(2,1)S(1)}, u32[]{:S(2)}, u32[]{:S(2)}) collective-permute-start(bf16[30,256]{1,0:T(8,128)(2,1)S(1)} %slice.266), channel_id=1, source_target_pairs={{0,4},{4,8},{8,12},{12,16},{16,20},{20,24},{24,28},{28,32},{32,36}... | collective-permute-start | bytes 46088 | tf_op jit(solution)/shard_map/ppermute | solution.py:12
  7.1 1.1 slice_convert_fusion.30
  8.2 0.8 copy.41
  9.6 1.0 slice_convert_fusion.29
  10.5 13.2 %collective-permute-done = bf16[30,256]{1,0:T(8,128)(2,1)S(1)} collective-permute-done((bf16[30,256]{1,0:T(8,128)(2,1)S(1)}, bf16[30,256]{1,0:T(8,128)(2,1)S(1)}, u32[]{:S(2)}, u32[]{:S(2)}) %collective-permute-start) | collective-permute-done | bytes 15392 | tf_op jit(solution)/shard_map/ppermute | solution.py:12
  23.8 3.2 fusion.52
  26.9 0.6 broadcast_in_dim.8
  27.5 3.3 %all-to-all-start = ((f32[4,1,1024]{2,1,0:T(1,128)}), f32[4,1,1024]{2,1,0:T(1,128)S(1)}, u32[]{:S(2)}, u32[]{:S(2)}) async-start(f32[4,1,1024]{2,1,0:T(1,128)} %broadcast_in_dim.8), calls=%async_computation | async-start | bytes 32768 | tf_op jit(solution)/shard_map/all_to_all | solution.py:17
  31.1 3.9 %all-to-all-done = f32[4,1,1024]{2,1,0:T(1,128)S(1)} async-done(((f32[4,1,1024]{2,1,0:T(1,128)}), f32[4,1,1024]{2,1,0:T(1,128)S(1)}, u32[]{:S(2)}, u32[]{:S(2)}) %all-to-all-start) | async-done | bytes 16416 | tf_op jit(solution)/shard_map/all_to_all | solution.py:17
  36.0 3.3 %all-to-all-start.1 = ((f32[4,1,512]{2,1,0:T(1,128)}), f32[4,1,512]{2,1,0:T(1,128)S(1)}, u32[]{:S(2)}, u32[]{:S(2)}) async-start(f32[4,1,512]{2,1,0:T(1,128)} %broadcast_in_dim.9), calls=%async_computation.1 | async-start | bytes 16384 | tf_op jit(solution)/shard_map/all_to_all | solution.py:17
  39.8 3.6 %all-to-all-done.1 = f32[4,1,512]{2,1,0:T(1,128)S(1)} async-done(((f32[4,1,512]{2,1,0:T(1,128)}), f32[4,1,512]{2,1,0:T(1,128)S(1)}, u32[]{:S(2)}, u32[]{:S(2)}) %all-to-all-start.1) | async-done | bytes 8224 | tf_op jit(solution)/shard_map/all_to_all | solution.py:17
  43.5 0.8 multiply_convert_fusion.1
  44.3 3.5 %all-to-all-start.2 = ((bf16[4,128,256]{2,1,0:T(8,128)(2,1)}), bf16[4,128,256]{2,1,0:T(8,128)(2,1)S(1)}, u32[]{:S(2)}, u32[]{:S(2)}) async-start(bf16[4,128,256]{2,1,0:T(8,128)(2,1)} %bitcast.31), calls=%async_computation.2 | async-start | bytes 524288 | tf_op jit(solution)/shard_map/all_to_all | solution.py:73
  47.9 5.4 %all-to-all-done.2 = bf16[4,128,256]{2,1,0:T(8,128)(2,1)S(1)} async-done(((bf16[4,128,256]{2,1,0:T(8,128)(2,1)}), bf16[4,128,256]{2,1,0:T(8,128)(2,1)S(1)}, u32[]{:S(2)}, u32[]{:S(2)}) %all-to-all-start.2) | async-done | bytes 262176 | tf_op jit(solution)/shard_map/all_to_all | solution.py:73
  53.5 3.1 multiply_reduce_fusion.1
  56.8 1.6 broadcast_in_dim.11
  58.4 2.3 reshape.156
  60.7 4.4 %scatter_custom_fusion = bf16[512,2048]{1,0:T(8,128)(2,1)} fusion(s32[256]{0:T(256)S(1)} %bitcast.97, bf16[256,2048]{1,0:T(8,128)(2,1)} %reshape.156, bf16[]{:T(256)} %constant.15.clone.1), kind=kCustom, calls=%fused_computation.46 | custom fusion | bytes 2097664 | tf_op jit(solution)/shard_map/scatter | solution.py:90
  65.1 4.1 %reshape.108 = bf16[128,4,2048]{2,1,0:T(4,128)(2,1)} reshape(bf16[512,2048]{1,0:T(8,128)(2,1)} %scatter_custom_fusion) | data formatting | bytes 4194304 | tf_op jit(solution)/shard_map/reshape | solution.py:92
  69.2 114.7 %all_to_all.41 = bf16[128,4,2048]{2,1,0:T(4,128)(2,1)} all-to-all(bf16[128,4,2048]{2,1,0:T(4,128)(2,1)} %reshape.108), channel_id=1, replica_groups=mesh['grp'=2,'sp'=32,'tp'=4] {'sp','tp'}, dimensions={0} | all-to-all | bytes 4194304 | tf_op jit(solution)/shard_map/all_to_all | solution.py:93
  183.9 4.0 %reshape.109 = bf16[512,2048]{1,0:T(8,128)(2,1)} reshape(bf16[128,4,2048]{2,1,0:T(4,128)(2,1)} %all_to_all.41) | data formatting | bytes 4194304 | tf_op jit(solution)/shard_map/reshape | solution.py:94
  187.9 4.4 %fusion.5 = f32[512,512]{1,0:T(8,128)} fusion(bf16[512,2048]{1,0:T(8,128)(2,1)} %reshape.109, bf16[1,2048,512]{2,1,0:T(8,128)(2,1)} %param.27), kind=kOutput, calls=%fused_computation.38 | convolution fusion | flops 1073741824 | bytes 5242880 | tf_op jit(solution)/shard_map/dot_general | solution.py:95
  192.3 6.2 %convolution_convert_fusion = bf16[512,2048]{1,0:T(8,128)(2,1)} fusion(bf16[1,512,2048]{2,1,0:T(8,128)(2,1)S(1)} %copy-done, bf16[512,2048]{1,0:T(8,128)(2,1)} %reshape.109, bf16[1,2048,512]{2,1,0:T(8,128)(2,1)} %param.28, f32[512,512]{1,0:T(8,128)} %fusion.5), kind=kOutput, calls=%fused_computation.31 | convolution fusion | flops 2150105088 | bytes 9437184 | tf_op jit(solution)/shard_map/dot_general | solution.py:98
  198.5 4.1 %reshape.110 = bf16[128,4,2048]{2,1,0:T(4,128)(2,1)} reshape(bf16[512,2048]{1,0:T(8,128)(2,1)} %convolution_convert_fusion) | data formatting | bytes 4194304 | tf_op jit(solution)/shard_map/reshape | solution.py:99
  202.6 10.0 %all-to-all-start.4 = ((bf16[128,4,2048]{2,1,0:T(4,128)(2,1)}), bf16[128,4,2048]{2,1,0:T(4,128)(2,1)}, u32[]{:S(2)}, u32[]{:S(2)}) async-start(bf16[128,4,2048]{2,1,0:T(4,128)(2,1)} %reshape.110), calls=%async_computation.4 | async-start | bytes 4194304 | tf_op jit(solution)/shard_map/all_to_all | solution.py:100
  212.8 97.7 %all-to-all-done.4 = bf16[128,4,2048]{2,1,0:T(4,128)(2,1)} async-done(((bf16[128,4,2048]{2,1,0:T(4,128)(2,1)}), bf16[128,4,2048]{2,1,0:T(4,128)(2,1)}, u32[]{:S(2)}, u32[]{:S(2)}) %all-to-all-start.4) | async-done | bytes 2097184 | tf_op jit(solution)/shard_map/all_to_all | solution.py:100
  310.6 4.0 %reshape.111 = bf16[512,2048]{1,0:T(8,128)(2,1)} reshape(bf16[128,4,2048]{2,1,0:T(4,128)(2,1)} %all-to-all-done.4) | data formatting | bytes 4194304 | tf_op jit(solution)/shard_map/reshape | solution.py:101
  314.5 5.2 %gather_fusion = bf16[256,2048]{1,0:T(8,128)(2,1)} fusion(bf16[512,2048]{1,0:T(8,128)(2,1)} %reshape.111, s32[1024]{0:T(1024)S(1)} %pad_clamp_fusion), kind=kCustom, calls=%fused_computation | custom fusion | bytes 2098176 | tf_op jit(solution)/shard_map/gather | solution.py:102
  319.7 3.4 %reshape.143 = f32[128,2,2048]{2,1,0:T(2,128)} reshape(bf16[256,2048]{1,0:T(8,128)(2,1)} %gather_fusion) | data formatting | bytes 3145728 | tf_op jit(solution)/shard_map/convert_element_type | solution.py:103
  323.1 4.8 %multiply_reduce_fusion = f32[128,2048]{1,0:T(8,128)S(1)} fusion(f32[128,2,2048]{2,1,0:T(2,128)} %reshape.143, f32[128,2]{1,0:T(8,128)S(1)} %copy.45), kind=kLoop, calls=%fused_computation.40 | loop fusion | flops 786432 | bytes 3146752 | tf_op jit(solution)/shard_map/reduce_sum | solution.py:103
  327.9 0.9 add_convert_fusion
  (41 shorter events, 2.7 us)
Async XLA Ops:
  0.0 192.3 %copy-start = (bf16[1,512,2048]{2,1,0:T(8,128)(2,1)S(1)}, bf16[1,512,2048]{2,1,0:T(8,128)(2,1)}, u32[]{:S(2)}) copy-start(bf16[1,512,2048]{2,1,0:T(8,128)(2,1)} %param.29) | copy-start | bytes 6291460
  0.0 30.9 %copy-start.2 = (s32[128,2]{0,1:T(2,128)S(1)}, s32[128,2]{0,1:T(2,128)}, u32[]{:S(2)}) copy-start(s32[128,2]{0,1:T(2,128)} %param.25) | copy-start | bytes 3076
  0.0 35.1 %copy-start.6 = (f32[256]{0:T(256)S(1)}, f32[256]{0:T(256)}, u32[]{:S(2)}) copy-start(f32[256]{0:T(256)} %param.19) | copy-start | bytes 3076
  0.0 35.1 %copy-start.5 = (f32[256]{0:T(256)S(1)}, f32[256]{0:T(256)}, u32[]{:S(2)}) copy-start(f32[256]{0:T(256)} %param.20) | copy-start | bytes 3076
  0.0 43.5 %copy-start.3 = (f32[256]{0:T(256)S(1)}, f32[256]{0:T(256)}, u32[]{:S(2)}) copy-start(f32[256]{0:T(256)} %param.21) | copy-start | bytes 3076
  1.4 22.4 %collective-permute-start = (bf16[30,256]{1,0:T(8,128)(2,1)S(1)}, bf16[30,256]{1,0:T(8,128)(2,1)S(1)}, u32[]{:S(2)}, u32[]{:S(2)}) collective-permute-start(bf16[30,256]{1,0:T(8,128)(2,1)S(1)} %slice.266), channel_id=1, source_target_pairs={{0,4},{4,8},{8,12},{12,16},{16,20},{20,24},{24,28},{28,32},{32,36}... | collective-permute-start | bytes 46088 | tf_op jit(solution)/shard_map/ppermute | solution.py:12
  27.5 7.5 %all-to-all-start = ((f32[4,1,1024]{2,1,0:T(1,128)}), f32[4,1,1024]{2,1,0:T(1,128)S(1)}, u32[]{:S(2)}, u32[]{:S(2)}) async-start(f32[4,1,1024]{2,1,0:T(1,128)} %broadcast_in_dim.8), calls=%async_computation | async-start | bytes 32768 | tf_op jit(solution)/shard_map/all_to_all | solution.py:17
  36.0 7.4 %all-to-all-start.1 = ((f32[4,1,512]{2,1,0:T(1,128)}), f32[4,1,512]{2,1,0:T(1,128)S(1)}, u32[]{:S(2)}, u32[]{:S(2)}) async-start(f32[4,1,512]{2,1,0:T(1,128)} %broadcast_in_dim.9), calls=%async_computation.1 | async-start | bytes 16384 | tf_op jit(solution)/shard_map/all_to_all | solution.py:17
  44.3 8.9 %all-to-all-start.2 = ((bf16[4,128,256]{2,1,0:T(8,128)(2,1)}), bf16[4,128,256]{2,1,0:T(8,128)(2,1)S(1)}, u32[]{:S(2)}, u32[]{:S(2)}) async-start(bf16[4,128,256]{2,1,0:T(8,128)(2,1)} %bitcast.31), calls=%async_computation.2 | async-start | bytes 524288 | tf_op jit(solution)/shard_map/all_to_all | solution.py:73
  53.5 3.2 copy-start.1
  202.6 10.0 %copy-start.4 = (f32[128,2]{0,1:T(2,128)S(1)}, f32[128,2]{0,1:T(2,128)}, u32[]{:S(2)}) copy-start(f32[128,2]{0,1:T(2,128)} %param.26) | copy-start | bytes 3076
  202.6 107.9 %all-to-all-start.4 = ((bf16[128,4,2048]{2,1,0:T(4,128)(2,1)}), bf16[128,4,2048]{2,1,0:T(4,128)(2,1)}, u32[]{:S(2)}, u32[]{:S(2)}) async-start(bf16[128,4,2048]{2,1,0:T(4,128)(2,1)} %reshape.110), calls=%async_computation.4 | async-start | bytes 4194304 | tf_op jit(solution)/shard_map/all_to_all | solution.py:100
where the time goes:
time: 330 us; the launch traced here: 329 us
  waiting for transfers between devices  124 us (38%)
  blocking collectives  115 us (35%)
  local copies, waits for them, and re-layouts  36 us (11%)
  starting transfers between devices  26 us (8%)
  other arithmetic  14.2 us (4%)
  matrix products  13.8 us (4%)
    all_to_all x1, blocking collectives, per_device(): lax.all_to_all(outgoing, ('sp', 'tp'), split_axis=0, concat_axis=0, tiled...  115 us
    all_to_all x1, waiting for transfers between devices, per_device(): lax.all_to_all(produced, ('sp', 'tp'), split_axis=0, concat_axis=0, tiled...  97.7 us
    ppermute x1, waiting for transfers between devices, passed_along(): return lax.ppermute(block, axis, route)  13.2 us
    all_to_all x1, starting transfers between devices, per_device(): lax.all_to_all(produced, ('sp', 'tp'), split_axis=0, concat_axis=0, tiled...  10 us
    all_to_all x2, waiting for transfers between devices, copy_for_each(): lax.all_to_all(jnp.broadcast_to(shard[None], (size, *shard.shape)), axis,...  7.57 us
    all_to_all x2, starting transfers between devices, copy_for_each(): lax.all_to_all(jnp.broadcast_to(shard[None], (size, *shard.shape)), axis,...  6.69 us
  transfers between devices with their start and end apart: 5, of which 5 were waited for; matrix products, arithmetic and copies ran while one was open for 1% of the time, Pallas kernels for 0%

commit v1 on v0

--- a/solution.py
+++ b/solution.py
@@ -70,7 +70,10 @@
         jnp.bfloat16
     )
     row_count = tok_rows // lax.axis_size("tp")
-    regrouped = lax.all_to_all(branch, "tp", split_axis=0, concat_axis=1, tiled=True)
+    regrouped = jnp.concatenate(
+        lax.all_to_all(jnp.stack(jnp.split(branch, lax.axis_size("tp"), axis=0)), "tp", 0, 0),
+        axis=1,
+    )
     projected = jnp.dot(regrouped, out_weight, preferred_element_type=jnp.float32)
     hidden = (residual.astype(jnp.float32) + projected).astype(jnp.bfloat16)
     widened = hidden.astype(jnp.float32)

time: 330 us -> 333 us (level)
  no operation moved by 1% of the time
where the time goes in v1:
time: 333 us; the launch traced here: 331 us
  waiting for transfers between devices  125 us (38%)
  blocking collectives  115 us (35%)
  local copies, waits for them, and re-layouts  38.3 us (12%)
  starting transfers between devices  26 us (8%)
  matrix products  13.8 us (4%)
  other arithmetic  13.3 us (4%)
    all_to_all x1, blocking collectives, per_device(): lax.all_to_all(outgoing, ('sp', 'tp'), split_axis=0, concat_axis=0, tiled...  115 us
    all_to_all x1, waiting for transfers between devices, per_device(): lax.all_to_all(produced, ('sp', 'tp'), split_axis=0, concat_axis=0, tiled...  97.7 us
    ppermute x1, waiting for transfers between devices, passed_along(): return lax.ppermute(block, axis, route)  14.2 us
    all_to_all x1, starting transfers between devices, per_device(): lax.all_to_all(produced, ('sp', 'tp'), split_axis=0, concat_axis=0, tiled...  10 us
    all_to_all x2, waiting for transfers between devices, copy_for_each(): lax.all_to_all(jnp.broadcast_to(shard[None], (size, *shard.shape)), axis,...  7.57 us
    all_to_all x2, starting transfers between devices, copy_for_each(): lax.all_to_all(jnp.broadcast_to(shard[None], (size, *shard.shape)), axis,...  6.69 us
  transfers between devices with their start and end apart: 5, of which 5 were waited for; matrix products, arithmetic and copies ran while one was open for 1% of the time, Pallas kernels for 0%

profile of v1, /device:TPU:33, one launch (start us, length us, event | category | flops | bytes accessed | tf_op | source)
XLA Modules:
  0.0 331.5 jit_solution(11082233588809008514)
XLA Ops:
  0.0 1.2 copy.33
  1.3 1.1 copy.34
  2.6 5.7 %collective-permute-start = (bf16[30,256]{0,1:T(8,128)(2,1)S(1)}, bf16[30,256]{0,1:T(8,128)(2,1)S(1)}, u32[]{:S(2)}, u32[]{:S(2)}) collective-permute-start(bf16[30,256]{0,1:T(8,128)(2,1)S(1)} %slice.266), channel_id=1, source_target_pairs={{0,4},{4,8},{8,12},{12,16},{16,20},{20,24},{24,28},{28,32},{32,36}... | collective-permute-start | bytes 46088 | tf_op jit(solution)/shard_map/ppermute | solution.py:12
  8.4 1.1 slice_convert_fusion.30
  9.5 0.8 copy.38
  10.9 14.2 %collective-permute-done = bf16[30,256]{0,1:T(8,128)(2,1)S(1)} collective-permute-done((bf16[30,256]{0,1:T(8,128)(2,1)S(1)}, bf16[30,256]{0,1:T(8,128)(2,1)S(1)}, u32[]{:S(2)}, u32[]{:S(2)}) %collective-permute-start) | collective-permute-done | bytes 15392 | tf_op jit(solution)/shard_map/ppermute | solution.py:12
  25.1 4.5 %fusion.52 = (f32[512]{0:T(512)S(1)}, f32[512]{0:T(512)S(1)}, f32[512,256]{0,1:T(8,128)S(1)}) fusion(f32[256]{0:T(256)S(1)} %bitcast.101, bf16[512,256]{0,1:T(8,128)(2,1)S(1)} %multiply_convert_fusion.2, f32[256]{0:T(256)S(1)} %bitcast.102, bf16[30,256]{0,1:T(8,128)(2,1)S(1)} %collective-permute-done, f32[256]{0:T(256)S(1)} %bitcast.73, ...), kind=kLoop, calls=%fused_computation.166 | loop fusion | flops 24378368 | bytes 838656 | tf_op jit(solution)/shard_map/reduce_sum | solution.py:64
  29.6 0.6 broadcast_in_dim.8
  30.2 3.3 %all-to-all-start = ((f32[4,1,1024]{2,1,0:T(1,128)}), f32[4,1,1024]{2,1,0:T(1,128)S(1)}, u32[]{:S(2)}, u32[]{:S(2)}) async-start(f32[4,1,1024]{2,1,0:T(1,128)} %broadcast_in_dim.8), calls=%async_computation | async-start | bytes 32768 | tf_op jit(solution)/shard_map/all_to_all | solution.py:17
  33.8 3.9 %all-to-all-done = f32[4,1,1024]{2,1,0:T(1,128)S(1)} async-done(((f32[4,1,1024]{2,1,0:T(1,128)}), f32[4,1,1024]{2,1,0:T(1,128)S(1)}, u32[]{:S(2)}, u32[]{:S(2)}) %all-to-all-start) | async-done | bytes 16416 | tf_op jit(solution)/shard_map/all_to_all | solution.py:17
  38.6 3.3 %all-to-all-start.1 = ((f32[4,1,512]{2,1,0:T(1,128)}), f32[4,1,512]{2,1,0:T(1,128)S(1)}, u32[]{:S(2)}, u32[]{:S(2)}) async-start(f32[4,1,512]{2,1,0:T(1,128)} %broadcast_in_dim.9), calls=%async_computation.1 | async-start | bytes 16384 | tf_op jit(solution)/shard_map/all_to_all | solution.py:17
  42.4 3.6 %all-to-all-done.1 = f32[4,1,512]{2,1,0:T(1,128)S(1)} async-done(((f32[4,1,512]{2,1,0:T(1,128)}), f32[4,1,512]{2,1,0:T(1,128)S(1)}, u32[]{:S(2)}, u32[]{:S(2)}) %all-to-all-start.1) | async-done | bytes 8224 | tf_op jit(solution)/shard_map/all_to_all | solution.py:17
  46.3 0.7 pad_maximum_fusion.1
  47.0 3.5 %all-to-all-start.2 = ((bf16[4,128,256]{1,2,0:T(8,128)(2,1)}), bf16[4,128,256]{1,2,0:T(8,128)(2,1)S(1)}, u32[]{:S(2)}, u32[]{:S(2)}) async-start(bf16[4,128,256]{1,2,0:T(8,128)(2,1)} %pad_maximum_fusion.1), calls=%async_computation.2 | async-start | bytes 524288 | tf_op jit(solution)/shard_map/all_to_all | solution.py:74
  50.5 5.4 %all-to-all-done.2 = bf16[4,128,256]{1,2,0:T(8,128)(2,1)S(1)} async-done(((bf16[4,128,256]{1,2,0:T(8,128)(2,1)}), bf16[4,128,256]{1,2,0:T(8,128)(2,1)S(1)}, u32[]{:S(2)}, u32[]{:S(2)}) %all-to-all-start.2) | async-done | bytes 262176 | tf_op jit(solution)/shard_map/all_to_all | solution.py:74
  56.0 3.1 multiply_reduce_fusion.1
  59.3 1.6 broadcast_in_dim.11
  60.9 2.3 reshape.161
  63.2 4.4 %scatter_custom_fusion = bf16[512,2048]{1,0:T(8,128)(2,1)} fusion(s32[256]{0:T(256)S(1)} %bitcast.104, bf16[256,2048]{1,0:T(8,128)(2,1)} %reshape.161, bf16[]{:T(256)} %constant.15.clone.1), kind=kCustom, calls=%fused_computation.46 | custom fusion | bytes 2097664 | tf_op jit(solution)/shard_map/scatter | solution.py:93
  67.6 4.1 %reshape.113 = bf16[128,4,2048]{2,1,0:T(4,128)(2,1)} reshape(bf16[512,2048]{1,0:T(8,128)(2,1)} %scatter_custom_fusion) | data formatting | bytes 4194304 | tf_op jit(solution)/shard_map/reshape | solution.py:95
  71.7 114.8 %all_to_all.27 = bf16[128,4,2048]{2,1,0:T(4,128)(2,1)} all-to-all(bf16[128,4,2048]{2,1,0:T(4,128)(2,1)} %reshape.113), channel_id=1, replica_groups=mesh['grp'=2,'sp'=32,'tp'=4] {'sp','tp'}, dimensions={0} | all-to-all | bytes 4194304 | tf_op jit(solution)/shard_map/all_to_all | solution.py:96
  186.5 4.0 %reshape.114 = bf16[512,2048]{1,0:T(8,128)(2,1)} reshape(bf16[128,4,2048]{2,1,0:T(4,128)(2,1)} %all_to_all.27) | data formatting | bytes 4194304 | tf_op jit(solution)/shard_map/reshape | solution.py:97
  190.5 4.5 %fusion.5 = f32[512,512]{1,0:T(8,128)} fusion(bf16[512,2048]{1,0:T(8,128)(2,1)} %reshape.114, bf16[1,2048,512]{2,1,0:T(8,128)(2,1)} %param.27), kind=kOutput, calls=%fused_computation.38 | convolution fusion | flops 1073741824 | bytes 5242880 | tf_op jit(solution)/shard_map/dot_general | solution.py:98
  194.9 6.2 %convolution_convert_fusion = bf16[512,2048]{1,0:T(8,128)(2,1)} fusion(bf16[1,512,2048]{2,1,0:T(8,128)(2,1)S(1)} %copy-done, bf16[512,2048]{1,0:T(8,128)(2,1)} %reshape.114, bf16[1,2048,512]{2,1,0:T(8,128)(2,1)} %param.28, f32[512,512]{1,0:T(8,128)} %fusion.5), kind=kOutput, calls=%fused_computation.2 | convolution fusion | flops 2150105088 | bytes 9437184 | tf_op jit(solution)/shard_map/dot_general | solution.py:101
  201.1 4.1 %reshape.115 = bf16[128,4,2048]{2,1,0:T(4,128)(2,1)} reshape(bf16[512,2048]{1,0:T(8,128)(2,1)} %convolution_convert_fusion) | data formatting | bytes 4194304 | tf_op jit(solution)/shard_map/reshape | solution.py:102
  205.2 10.0 %all-to-all-start.4 = ((bf16[128,4,2048]{2,1,0:T(4,128)(2,1)}), bf16[128,4,2048]{2,1,0:T(4,128)(2,1)}, u32[]{:S(2)}, u32[]{:S(2)}) async-start(bf16[128,4,2048]{2,1,0:T(4,128)(2,1)} %reshape.115), calls=%async_computation.4 | async-start | bytes 4194304 | tf_op jit(solution)/shard_map/all_to_all | solution.py:103
  215.4 97.7 %all-to-all-done.4 = bf16[128,4,2048]{2,1,0:T(4,128)(2,1)} async-done(((bf16[128,4,2048]{2,1,0:T(4,128)(2,1)}), bf16[128,4,2048]{2,1,0:T(4,128)(2,1)}, u32[]{:S(2)}, u32[]{:S(2)}) %all-to-all-start.4) | async-done | bytes 2097184 | tf_op jit(solution)/shard_map/all_to_all | solution.py:103
  313.1 4.0 %reshape.116 = bf16[512,2048]{1,0:T(8,128)(2,1)} reshape(bf16[128,4,2048]{2,1,0:T(4,128)(2,1)} %all-to-all-done.4) | data formatting | bytes 4194304 | tf_op jit(solution)/shard_map/reshape | solution.py:104
  317.1 5.2 %gather_fusion = bf16[256,2048]{1,0:T(8,128)(2,1)} fusion(bf16[512,2048]{1,0:T(8,128)(2,1)} %reshape.116, s32[1024]{0:T(1024)S(1)} %pad_clamp_fusion), kind=kCustom, calls=%fused_computation | custom fusion | bytes 2098176 | tf_op jit(solution)/shard_map/gather | solution.py:105
  322.3 3.4 %reshape.148 = f32[128,2,2048]{2,1,0:T(2,128)} reshape(bf16[256,2048]{1,0:T(8,128)(2,1)} %gather_fusion) | data formatting | bytes 3145728 | tf_op jit(solution)/shard_map/convert_element_type | solution.py:106
  325.7 4.8 %multiply_reduce_fusion = f32[128,2048]{1,0:T(8,128)S(1)} fusion(f32[128,2,2048]{2,1,0:T(2,128)} %reshape.148, f32[128,2]{1,0:T(8,128)S(1)} %copy.42), kind=kLoop, calls=%fused_computation.40 | loop fusion | flops 786432 | bytes 3146752 | tf_op jit(solution)/shard_map/reduce_sum | solution.py:106
  330.5 0.9 add_convert_fusion
  (48 shorter events, 2.8 us)
Async XLA Ops:
  0.0 194.9 %copy-start = (bf16[1,512,2048]{2,1,0:T(8,128)(2,1)S(1)}, bf16[1,512,2048]{2,1,0:T(8,128)(2,1)}, u32[]{:S(2)}) copy-start(bf16[1,512,2048]{2,1,0:T(8,128)(2,1)} %param.29) | copy-start | bytes 6291460
  0.0 10.8 %copy-start.1 = (bf16[31,256]{1,0:T(8,128)(2,1)S(1)}, bf16[31,256]{1,0:T(8,128)(2,1)}, u32[]{:S(2)}) copy-start(bf16[31,256]{1,0:T(8,128)(2,1)} %param.17) | copy-start | bytes 47620
  0.0 33.6 %copy-start.3 = (s32[128,2]{0,1:T(2,128)S(1)}, s32[128,2]{0,1:T(2,128)}, u32[]{:S(2)}) copy-start(s32[128,2]{0,1:T(2,128)} %param.25) | copy-start | bytes 3076
  0.0 25.1 %copy-start.4 = (f32[256]{0:T(256)S(1)}, f32[256]{0:T(256)}, u32[]{:S(2)}) copy-start(f32[256]{0:T(256)} %param.18) | copy-start | bytes 3076
  0.0 37.7 %copy-start.8 = (f32[256]{0:T(256)S(1)}, f32[256]{0:T(256)}, u32[]{:S(2)}) copy-start(f32[256]{0:T(256)} %param.19) | copy-start | bytes 3076
  0.0 37.7 %copy-start.7 = (f32[256]{0:T(256)S(1)}, f32[256]{0:T(256)}, u32[]{:S(2)}) copy-start(f32[256]{0:T(256)} %param.20) | copy-start | bytes 3076
  2.4 43.7 %copy-start.5 = (f32[256]{0:T(256)S(1)}, f32[256]{0:T(256)}, u32[]{:S(2)}) copy-start(f32[256]{0:T(256)} %param.21) | copy-start | bytes 3076
  2.6 22.4 %collective-permute-start = (bf16[30,256]{0,1:T(8,128)(2,1)S(1)}, bf16[30,256]{0,1:T(8,128)(2,1)S(1)}, u32[]{:S(2)}, u32[]{:S(2)}) collective-permute-start(bf16[30,256]{0,1:T(8,128)(2,1)S(1)} %slice.266), channel_id=1, source_target_pairs={{0,4},{4,8},{8,12},{12,16},{16,20},{20,24},{24,28},{28,32},{32,36}... | collective-permute-start | bytes 46088 | tf_op jit(solution)/shard_map/ppermute | solution.py:12
  30.2 7.5 %all-to-all-start = ((f32[4,1,1024]{2,1,0:T(1,128)}), f32[4,1,1024]{2,1,0:T(1,128)S(1)}, u32[]{:S(2)}, u32[]{:S(2)}) async-start(f32[4,1,1024]{2,1,0:T(1,128)} %broadcast_in_dim.8), calls=%async_computation | async-start | bytes 32768 | tf_op jit(solution)/shard_map/all_to_all | solution.py:17
  38.6 7.4 %all-to-all-start.1 = ((f32[4,1,512]{2,1,0:T(1,128)}), f32[4,1,512]{2,1,0:T(1,128)S(1)}, u32[]{:S(2)}, u32[]{:S(2)}) async-start(f32[4,1,512]{2,1,0:T(1,128)} %broadcast_in_dim.9), calls=%async_computation.1 | async-start | bytes 16384 | tf_op jit(solution)/shard_map/all_to_all | solution.py:17
  47.0 8.9 %all-to-all-start.2 = ((bf16[4,128,256]{1,2,0:T(8,128)(2,1)}), bf16[4,128,256]{1,2,0:T(8,128)(2,1)S(1)}, u32[]{:S(2)}, u32[]{:S(2)}) async-start(bf16[4,128,256]{1,2,0:T(8,128)(2,1)} %pad_maximum_fusion.1), calls=%async_computation.2 | async-start | bytes 524288 | tf_op jit(solution)/shard_map/all_to_all | solution.py:74
  56.0 3.1 copy-start.2
  205.2 10.0 %copy-start.6 = (f32[128,2]{0,1:T(2,128)S(1)}, f32[128,2]{0,1:T(2,128)}, u32[]{:S(2)}) copy-start(f32[128,2]{0,1:T(2,128)} %param.26) | copy-start | bytes 3076
  205.2 107.9 %all-to-all-start.4 = ((bf16[128,4,2048]{2,1,0:T(4,128)(2,1)}), bf16[128,4,2048]{2,1,0:T(4,128)(2,1)}, u32[]{:S(2)}, u32[]{:S(2)}) async-start(bf16[128,4,2048]{2,1,0:T(4,128)(2,1)} %reshape.115), calls=%async_computation.4 | async-start | bytes 4194304 | tf_op jit(solution)/shard_map/all_to_all | solution.py:103
